TPU v7x, 32 devices: a whole 2x2x4 slice. The times are simulated.
32 devices in a mesh: sp: 16 (over z, y, x), tp: 2 (over core).
Axes of the slice: x: 2, y: 2, z: 4, core: 2. Of those that a mesh axis runs over, the one named last changes fastest.
Arguments:
- tokens: bfloat16 [4096, 2048], P('sp', 'tp'), may hold values from -6 to 6
- norm_gain: float32 [2, 2048], replicated, may hold values from 0.1 to 1.9
- w_bgate: bfloat16 [2, 2048, 2048], P(None, 'sp', 'tp'), may hold values from -0.125 to 0.125
- w_cgate: bfloat16 [2, 2048, 2048], P(None, 'sp', 'tp'), may hold values from -0.125 to 0.125
- w_value: bfloat16 [2, 2048, 2048], P(None, 'sp', 'tp'), may hold values from -0.125 to 0.125
- conv_taps: float32 [2, 3, 2048], replicated, may hold values from -3.5 to 3.5
- w_out: bfloat16 [2, 2048, 2048], P(None, 'sp', 'tp'), may hold values from -0.125 to 0.125
Outputs:
- mixed_out: bfloat16 [4096, 2048], P('sp', 'tp')
All inputs are finite; a program needn't handle non-finite values.
Results may differ from a plain program's by a relative error of at most 0.015.
Values may be sent and summed in bfloat16 or wider, within the bound.
A program may use at most 64 MiB of HBM per device.

v0:
```python
import functools

import jax
import jax.numpy as jnp
from jax import lax
from jax.experimental import pallas as pl
from jax.experimental.pallas import tpu as pltpu
from jax.sharding import PartitionSpec as P

MESH = pl.DeviceIdType.MESH
LANES = 128
AHEAD = 2
BEFORE_TOKENS = 2
F32 = jnp.float32
BF16 = jnp.bfloat16


def mixer_kernel(dims, tok, gain, wb, wc, wv, taps, wo, out,
                 acts, gates, normed, weights, product, cgate, result, landed,
                 loc_sem, plane_send, plane_recv, line_send, line_recv,
                 ag_send, ag_recv, pair_send, pair_recv,
                 halo_send, halo_recv, out_send, out_recv):
    depth, group, line, tps, rows, cols, width, krows = dims
    span = rows * group
    block = krows * group
    chunks = [(l, m) for l in range(depth) for m in range(4)]
    sources = (wc, wv, wb, wo)
    sp, t = lax.axis_index("sp"), lax.axis_index("tp")
    z, q = sp // group, sp % group
    own = pl.multiple_of(t * cols + q * width, width)
    tile = min(256, rows)

    def in_plane(d):
        return (z * group + (q + d) % group, t)

    def in_pair(d):
        return (sp, (t + d) % tps)

    def remote(src, dst, send, recv, device):
        return pltpu.make_async_remote_copy(src_ref=src, dst_ref=dst, send_sem=send, recv_sem=recv,
                                            device_id=device, device_id_type=MESH)

    barrier = pltpu.get_barrier_semaphore()

    def hello(device):
        pl.semaphore_signal(barrier, inc=1, device_id=device, device_id_type=MESH)

    for d in range(1, group):
        hello(in_plane(d))
    for d in range(1, tps):
        hello(in_pair(d))

    @pl.when(z > 0)
    def _():
        hello((sp - group, t))

    @pl.when(z < line - 1)
    def _():
        hello((sp + group, t))

    pl.semaphore_wait(barrier, group - 1 + tps - 1
                      + jnp.where(z > 0, 1, 0) + jnp.where(z < line - 1, 1, 0))

    def weight_rows(i, zz, qq):
        l, m = chunks[i]
        return weights.at[l, m, pl.ds(pl.multiple_of((zz * group + qq) * krows, krows), krows), :]

    def weight_block(i, zz):
        l, m = chunks[i]
        return weights.at[l, m, pl.ds(pl.multiple_of(zz * block, block), block), :]

    def weight_source(i, qq):
        l, m = chunks[i]
        return sources[m].at[l, :, pl.ds(pl.multiple_of(qq * width, width), width)]

    def plane_copy(i, d, sender):
        return remote(weight_source(i, (q + d) % group), weight_rows(i, z, sender),
                      plane_send.at[i, d], plane_recv.at[i, d], in_plane(d))

    def local_copy(i):
        return pltpu.make_async_copy(weight_source(i, q), weight_rows(i, z, q), loc_sem.at[i])

    def line_copy(i, zz, up):
        blk = weight_block(i, zz)
        return remote(blk, blk, line_send.at[0 if up else 1, i, zz], line_recv.at[i, zz],
                      (sp + group, t) if up else (sp - group, t))

    def plane_start(i):
        local_copy(i).start()
        for d in range(1, group):
            plane_copy(i, d, q).start()

    def line_start(i):
        local_copy(i).wait()
        for d in range(1, group):
            plane_copy(i, d, (q + group - d) % group).wait_recv()

        @pl.when(z < line - 1)
        def _():
            line_copy(i, z, True).start()

        @pl.when(z > 0)
        def _():
            line_copy(i, z, False).start()

    def line_round(i):
        def step(j, carry):
            below, above = z - 1 - j, z + 1 + j

            @pl.when(below >= 0)
            def _():
                line_copy(i, below, True).wait_recv()

                @pl.when(z < line - 1)
                def _():
                    line_copy(i, below, True).start()

            @pl.when(above < line)
            def _():
                line_copy(i, above, False).wait_recv()

                @pl.when(z > 0)
                def _():
                    line_copy(i, above, False).start()

            return carry

        lax.fori_loop(0, line - 1, step, 0)
        if i + AHEAD < len(chunks) - 1:
            line_start(i + AHEAD)
        if i == len(chunks) - 2:
            line_start(i + 1)

    def act_half(ph, tt, qq, h):
        if ph == 0:
            part = rows // 2
            return acts.at[0, pl.ds(pl.multiple_of(qq * rows + h * part, part), part),
                           pl.ds(pl.multiple_of(tt * cols, cols), cols)]
        part = span // 2
        buf = acts if ph % 2 == 0 else gates
        return buf.at[ph // 2, pl.ds(h * part, part),
                      pl.ds(pl.multiple_of(tt * cols + qq * width, width), width)]

    def own_half(ph, h):
        if ph == 0:
            return tok.at[pl.ds(h * (rows // 2), rows // 2), :]
        return act_half(ph, t, q, h)

    def flip(qq, bits):
        if bits & 1:
            qq = qq + 1 - 2 * (qq % 2)
        if bits & 2:
            qq = qq + 2 - 4 * ((qq // 2) % 2)
        return qq

    directs = ([(1, 0), (1, 1)] if group >= 2 else []) + ([(2, 1), (2, 0)] if group >= 4 else [])
    relays = [(1, 0, 2), (2, 1, 1)] if group >= 4 else []

    def direct_copy(ph, bits, h, sending):
        src = own_half(ph, h)
        dst = act_half(ph, t, q if sending else flip(q, bits), h)
        return remote(src, dst, ag_send.at[ph, bits, h], ag_recv.at[ph, bits, h],
                      (z * group + flip(q, bits), t))

    def relay_copy(ph, origin, h, to, sending):
        part = act_half(ph, t, flip(q, origin if sending else 3), h)
        return remote(part, part, ag_send.at[ph, 3, h], ag_recv.at[ph, 3, h],
                      (z * group + flip(q, to), t))

    def pair_copy(ph, bits, h, d, tt):
        qq = flip(q, bits)
        src = own_half(ph, h) if bits == 0 else act_half(ph, t, qq, h)
        return remote(src, act_half(ph, tt, qq, h), pair_send.at[ph, bits, h, d],
                      pair_recv.at[ph, bits, h, d], in_pair(d))

    def pair_start(ph, bits, h):
        for d in range(1, tps):
            pair_copy(ph, bits, h, d, t).start()

    def gather_start(ph):
        for bits, h in directs:
            direct_copy(ph, bits, h, True).start()
        for h in range(2):
            pair_start(ph, 0, h)

    def gather_relay(ph):
        for origin, h, to in relays:
            direct_copy(ph, origin, h, False).wait_recv()
            relay_copy(ph, origin, h, to, True).start()
        for origin, h, to in relays:
            pair_start(ph, origin, h)

    def gather_finish(ph):
        relayed = [(origin, h) for origin, h, _ in relays]
        for bits, h in directs:
            if (bits, h) not in relayed:
                direct_copy(ph, bits, h, False).wait_recv()
                pair_start(ph, bits, h)
        for origin, h, to in relays:
            relay_copy(ph, origin, h, to, False).wait_recv()
            pair_start(ph, 3, h)
        for bits in range(group):
            for h in range(2):
                for d in range(1, tps):
                    pair_copy(ph, bits, h, d, (t + tps - d) % tps).wait_recv()

    def tiles(body):
        def step(i, carry):
            body(pl.multiple_of(i * tile, tile))
            return carry

        lax.fori_loop(0, span // tile, step, 0)

    def normalize(l):
        sub = 128

        def step(i, carry):
            at = pl.ds(pl.multiple_of(i * sub, sub), sub)
            x = acts[l, at, :].astype(F32)
            scale = lax.rsqrt(jnp.mean(x * x, axis=-1, keepdims=True) + 1e-06)
            normed[at, :] = (x * scale * gain[pl.ds(l, 1), :]).astype(BF16)
            return carry

        lax.fori_loop(0, span // sub, step, 0)

    def project(l, m, r):
        return jnp.dot(normed[pl.ds(r, tile), :], weights[l, m], preferred_element_type=F32).astype(BF16)

    def halo_copy(l):
        return remote(product.at[l, pl.ds(span, 8), :], product.at[l, pl.ds(0, 8), :],
                      halo_send.at[l], halo_recv.at[l], (sp + group, t))

    def do_cgate(l):
        def body(r):
            cgate[pl.ds(r, tile), :] = project(l, 0, r)
        tiles(body)

    def do_values(l):
        def body(r):
            values = project(l, 1, r)
            product[l, pl.ds(r + 8, tile), :] = cgate[pl.ds(r, tile), :].astype(F32) * values.astype(F32)
        tiles(body)

        @pl.when(z < line - 1)
        def _():
            halo_copy(l).start()

    def do_bgate(l):
        @pl.when(z > 0)
        def _():
            halo_copy(l).wait_recv()

        @pl.when(z == 0)
        def _():
            product[l, pl.ds(0, 8), :] = jnp.zeros((8, width), F32)

        tap = [taps[l, pl.ds(k, 1), pl.ds(own, width)] for k in range(3)]

        def body(r):
            bgate = project(l, 2, r).astype(F32)
            near = product[l, pl.ds(r, tile + 8), :]
            mixed = tap[0] * near[6:6 + tile] + tap[1] * near[7:7 + tile] + tap[2] * near[8:8 + tile]
            gates[l, pl.ds(r, tile), pl.ds(own, width)] = (bgate * mixed).astype(BF16)
        tiles(body)

    def out_tile(l):
        def body(r):
            update = jnp.dot(gates[l, pl.ds(r, tile), :], weights[l, 3], preferred_element_type=F32)
            current = (acts[l, pl.ds(r, tile), pl.ds(own, width)].astype(F32) + update).astype(BF16)
            if l + 1 < depth:
                acts[l + 1, pl.ds(r, tile), pl.ds(own, width)] = current
            else:
                result[pl.ds(r, tile), :] = current
        return body

    def do_out(l):
        tiles(out_tile(l))

    def do_out_rows(l, qq):
        body = out_tile(l)
        for k in range(rows // tile):
            body(pl.multiple_of(qq * rows + k * tile, tile))

    def out_copy(d, qq):
        return remote(result.at[pl.ds(pl.multiple_of((q + d) % group * rows, rows), rows), :],
                      landed.at[:, pl.ds(pl.multiple_of(qq * width, width), width)],
                      out_send.at[d], out_recv.at[d], in_plane(d))

    own_tokens = pltpu.make_async_copy(tok, acts.at[0, pl.ds(pl.multiple_of(q * rows, rows), rows), pl.ds(pl.multiple_of(t * cols, cols), cols)], loc_sem.at[len(chunks)])
    own_tokens.start()
    for i in range(len(chunks)):
        if i == min(BEFORE_TOKENS, len(chunks) - 1):
            gather_start(0)
        plane_start(i)
    for i in range(min(AHEAD, len(chunks))):
        line_start(i)
    line_round(0)
    gather_relay(0)
    own_tokens.wait()
    for l in range(depth):
        gather_finish(2 * l)
        normalize(l)
        do_cgate(l)
        if l == 0:
            line_round(1)
        do_values(l)
        line_round(4 * l + 2)
        do_bgate(l)
        gather_start(2 * l + 1)
        gather_relay(2 * l + 1)
        line_round(4 * l + 3)
        gather_finish(2 * l + 1)
        if l + 1 < depth:
            do_out(l)
            line_round(4 * l + 4)
            gather_start(2 * l + 2)
            gather_relay(2 * l + 2)
            line_round(4 * l + 5)
    for d in range(1, group + 1):
        do_out_rows(depth - 1, (q + d) % group)
        if d > 1:
            out_copy(d - 1, q).start()
    landed[:, pl.ds(pl.multiple_of(q * width, width), width)] = result[
        pl.ds(pl.multiple_of(q * rows, rows), rows), :]
    for d in range(1, group):
        out_copy(d, (q + group - d) % group).wait_recv()
    out[...] = landed[...]

    for i in range(len(chunks)):
        for d in range(1, group):
            plane_copy(i, d, q).wait_send()

        def step(zz, carry):
            @pl.when((z < line - 1) & (zz <= z))
            def _():
                line_copy(i, zz, True).wait_send()

            @pl.when((z > 0) & (zz >= z))
            def _():
                line_copy(i, zz, False).wait_send()

            return carry

        lax.fori_loop(0, line, step, 0)
    for ph in range(2 * depth):
        for bits, h in directs:
            direct_copy(ph, bits, h, True).wait_send()
        for origin, h, to in relays:
            relay_copy(ph, origin, h, to, True).wait_send()
        for bits in range(group):
            for h in range(2):
                for d in range(1, tps):
                    pair_copy(ph, bits, h, d, t).wait_send()
    for l in range(depth):
        @pl.when(z < line - 1)
        def _():
            halo_copy(l).wait_send()
    for d in range(1, group):
        out_copy(d, q).wait_send()


def shards(sp_size, tps, tokens, norm_gain, w_bgate, w_cgate, w_value, conv_taps, w_out):
    rows, cols = tokens.shape
    depth, krows, _ = w_bgate.shape
    group = 4
    while group > 1 and (sp_size % group or cols % (group * LANES)):
        group //= 2
    line = sp_size // group
    width = cols // group
    span = rows * group
    full = krows * sp_size
    n = 4 * depth
    dims = (depth, group, line, tps, rows, cols, width, krows)
    anywhere = pl.BlockSpec(memory_space=pl.ANY)
    vmem = pl.BlockSpec(memory_space=pltpu.VMEM)
    dma = pltpu.SemaphoreType.DMA
    return pl.pallas_call(
        functools.partial(mixer_kernel, dims),
        out_shape=jax.ShapeDtypeStruct((rows, cols), BF16),
        in_specs=[anywhere, vmem, anywhere, anywhere, anywhere, vmem, anywhere],
        out_specs=vmem,
        scratch_shapes=[
            pltpu.VMEM((depth, span, full), BF16),
            pltpu.VMEM((depth, span, full), BF16),
            pltpu.VMEM((span, full), BF16),
            pltpu.VMEM((depth, 4, full, width), BF16),
            pltpu.VMEM((depth, span + 8, width), F32),
            pltpu.VMEM((span, width), BF16),
            pltpu.VMEM((span, width), BF16),
            pltpu.VMEM((rows, cols), BF16),
            dma((n + 1,)), dma((n, group)), dma((n, group)),
            dma((2, n, line)), dma((n, line)),
            dma((2 * depth, 4, 2)), dma((2 * depth, 4, 2)),
            dma((2 * depth, group, 2, tps)), dma((2 * depth, group, 2, tps)),
            dma((depth,)), dma((depth,)), dma((group,)), dma((group,)),
        ],
        compiler_params=pltpu.CompilerParams(
            collective_id=0, has_side_effects=True, vmem_limit_bytes=60 * 1024 * 1024),
    )(tokens, norm_gain, w_bgate, w_cgate, w_value, conv_taps, w_out)


def solution(mesh):
    return jax.shard_map(
        functools.partial(shards, mesh.shape["sp"], mesh.shape["tp"]),
        mesh=mesh,
        in_specs=(
            P("sp", "tp"),
            P(),
            P(None, "sp", "tp"),
            P(None, "sp", "tp"),
            P(None, "sp", "tp"),
            P(),
            P(None, "sp", "tp"),
        ),
        out_specs=P("sp", "tp"),
        check_vma=False,
    )
```

profile of v0, /device:TPU:0, one launch (start us, length us, event | category | flops | bytes accessed | tf_op | source)
XLA Modules:
  0.0 186.3 jit_solution(6244033114683298686)
XLA Ops:
  0.0 1.5 copy.8.taps
  1.5 183.0 %shard_map.73 = bf16[256,1024]{1,0:T(8,128)(2,1)} custom-call(bf16[256,1024]{1,0:T(8,128)(2,1)} %tok.1, f32[2,2048]{1,0:T(2,128)} %gain.1, bf16[2,128,1024]{2,1,0:T(8,128)(2,1)} %wb.1, bf16[2,128,1024]{2,1,0:T(8,128)(2,1)} %wc.1, bf16[2,128,1024]{2,1,0:T(8,128)(2,1)} %wv.1, f32[2,3,2048]{2,1,0:T(4,128)} %copy.8.taps, bf16[2,128,1024]{2,1,0:T(8,128)(2,1)} %wo.1), custom_call_target="tpu_custom_call" | custom-call | tf_op jit(solution)/shard_map/pallas_call | solution.py:377
  184.4 1.9 %copy.10 = bf16[256,1024]{1,0:T(8,128)(2,1)} copy(bf16[256,1024]{1,0:T(8,128)(2,1)} %shard_map.73) | data formatting | bytes 1048576
where the time goes:
time: 187 us; the launch traced here: 186 us
  Pallas kernels  183 us (98%)
  local copies, waits for them, and re-layouts  3.33 us (2%)
    pallas_call x1, Pallas kernels, shards(): pl.pallas_call(functools.partial(mixer_kernel, dims), out_shape=jax.Shape...  183 us

commit v1 on v0

v1 whole, which is shorter than its diff:
```python
import functools

import jax
import jax.numpy as jnp
from jax import lax
from jax.experimental import pallas as pl
from jax.experimental.pallas import tpu as pltpu
from jax.sharding import PartitionSpec as P

MESH = pl.DeviceIdType.MESH
LANES = 128
AHEAD = 2
PIECES = 4
F32 = jnp.float32
BF16 = jnp.bfloat16


def mixer_kernel(dims, tok, gain, wb, wc, wv, taps, wo, out,
                 acts, gates, normed, weights, product, cgate, gsend, result, landed,
                 loc_sem, plane_send, plane_recv, line_send, line_recv,
                 ag_send, ag_recv, pair_send, pair_recv,
                 halo_send, halo_recv, out_send, out_recv,
                 tok_send, tok_recv, gate_send, gate_recv,
                 raw, raw_send, raw_recv, guest_send, guest_recv):
    depth, group, line, tps, rows, cols, width, krows = dims
    span = rows * group
    block = krows * group
    tile = span // PIECES
    lend = line >= 4
    guest = depth
    chunks = [(l, m) for l in range(depth) for m in range(4)]
    last = len(chunks)
    sources = (wc, wv, wb, wo)
    sp, t = lax.axis_index("sp"), lax.axis_index("tp")
    z, q = sp // group, sp % group
    own = pl.multiple_of(t * cols + q * width, width)
    end = (z == 0) | (z == line - 1)
    host = (z == 1) | (z == line - 2)
    partner = jnp.where((z == 0) | (z == line - 2), sp + group, sp - group)

    def only(cond, body):
        if lend:
            pl.when(cond)(body)

    def unless_end(body):
        if lend:
            pl.when(jnp.logical_not(end))(body)
        else:
            body()

    def in_plane(d):
        return (z * group + (q + d) % group, t)

    def in_pair(d):
        return (sp, (t + d) % tps)

    def remote(src, dst, send, recv, device):
        return pltpu.make_async_remote_copy(src_ref=src, dst_ref=dst, send_sem=send, recv_sem=recv,
                                            device_id=device, device_id_type=MESH)

    def each(body):
        def step(p, carry):
            body(p)
            return carry

        lax.fori_loop(0, PIECES, step, 0)

    barrier = pltpu.get_barrier_semaphore()

    def hello(device):
        pl.semaphore_signal(barrier, inc=1, device_id=device, device_id_type=MESH)

    for d in range(1, group):
        hello(in_plane(d))
    for d in range(1, tps):
        hello(in_pair(d))

    @pl.when(z > 0)
    def _():
        hello((sp - group, t))

    @pl.when(z < line - 1)
    def _():
        hello((sp + group, t))

    pl.semaphore_wait(barrier, group - 1 + tps - 1
                      + jnp.where(z > 0, 1, 0) + jnp.where(z < line - 1, 1, 0))

    def weight_rows(i, zz, qq):
        l, m = chunks[i]
        return weights.at[l, m, pl.ds(pl.multiple_of((zz * group + qq) * krows, krows), krows), :]

    def weight_block(i, zz):
        l, m = chunks[i]
        return weights.at[l, m, pl.ds(pl.multiple_of(zz * block, block), block), :]

    def weight_source(i, qq):
        l, m = chunks[i]
        return sources[m].at[l, :, pl.ds(pl.multiple_of(qq * width, width), width)]

    def plane_copy(i, d, sender):
        return remote(weight_source(i, (q + d) % group), weight_rows(i, z, sender),
                      plane_send.at[i, d], plane_recv.at[i, d], in_plane(d))

    def local_copy(i):
        return pltpu.make_async_copy(weight_source(i, q), weight_rows(i, z, q), loc_sem.at[i])

    low = 2 * z < line

    def line_copy(i, zz, up):
        blk = weight_block(i, zz)
        return remote(blk, blk, line_send.at[jnp.where(up, 0, 1), i, zz], line_recv.at[i, zz],
                      (jnp.where(up, sp + group, sp - group), t))

    def lent(i):
        l, m = chunks[i]
        return lend and l == 0 and m < 3

    def reach(i):
        return (1, line - 2) if lent(i) else (0, line - 1)

    def goes(i, zz, up):
        lo, hi = reach(i)
        on = jnp.where(up, z < hi, z > lo)
        if lend and not lent(i):
            on = on & jnp.logical_not((zz == z) & (jnp.where(up, z, line - 1 - z) == line - 2))
        return on

    def plane_start(i):
        local_copy(i).start()
        for d in range(1, group):
            plane_copy(i, d, q).start()

    def line_start(i):
        local_copy(i).wait()
        for d in range(1, group):
            plane_copy(i, d, (q + group - d) % group).wait_recv()
        for up in (low, jnp.logical_not(low)):
            @pl.when(goes(i, z, up))
            def _():
                line_copy(i, z, up).start()

    def line_pass(i, up):
        lo, hi = reach(i)

        def step(j, carry):
            zz = jnp.where(up, z - 1 - j, z + 1 + j)
            here = (zz >= 0) & (zz < line) & (z >= lo) & (z <= hi)
            if lend and not lent(i):
                here = here & jnp.logical_not(end & (zz == jnp.where(z == 0, 1, line - 2)))

            @pl.when(here)
            def _():
                line_copy(i, zz, up).wait_recv()

                @pl.when(goes(i, zz, up))
                def _():
                    line_copy(i, zz, up).start()

            return carry

        lax.fori_loop(0, line - 1, step, 0)

    def inward(i):
        line_pass(i, low)

    def outward(i):
        line_pass(i, jnp.logical_not(low))
        if lend and not lent(i):
            @functools.partial(only, end)
            def _():
                for d in range(1, group):
                    guest_copy(i, d, (q + group - d) % group).wait_recv()

    def raw_copy(i, d):
        dst = weight_rows(i, z, q) if d == 0 else raw.at[i, d - 1]
        return remote(weight_source(i, (q + d) % group), dst, raw_send.at[i, d], raw_recv.at[i, d], (partner, t))

    def host_z():
        return jnp.where(z == 0, 1, line - 2)

    def guest_copy(i, d, sender):
        return remote(raw.at[i, d - 1], weight_rows(i, host_z(), sender),
                      guest_send.at[i, d], guest_recv.at[i, d], in_plane(d))

    def raw_take(i):
        for d in range(group):
            if d == 0:
                remote(weight_source(i, q), weight_rows(i, host_z(), q), raw_send.at[i, 0], raw_recv.at[i, 0],
                       (partner, t)).wait_recv()
            else:
                raw_copy(i, d).wait_recv()
                guest_copy(i, d, q).start()

    by_rows = (0, 2 * depth)

    def piece(ph, tt, qq, p, sub=None):
        if ph in by_rows:
            part, slot = rows // PIECES, 0 if ph == 0 else guest
            first, col, wide, buf = qq * rows, tt * cols, cols, acts
        else:
            part, slot = tile, ph // 2
            first, col, wide, buf = 0, tt * cols + qq * width, width, acts if ph % 2 == 0 else gates
        size = part if sub is None else part // 2
        at = first + p * part + (0 if sub is None else sub * size)
        return buf.at[slot, pl.ds(pl.multiple_of(at, size), size), pl.ds(pl.multiple_of(col, wide), wide)]

    def own_piece(ph, p):
        if ph == 0:
            part = rows // PIECES
            return tok.at[pl.ds(pl.multiple_of(p * part, part), part), :]
        return piece(ph, t, q, p)

    def flip(qq, bits):
        if bits & 1:
            qq = qq + 1 - 2 * (qq % 2)
        if bits & 2:
            qq = qq + 2 - 4 * ((qq // 2) % 2)
        return qq

    directs = ([1] if group >= 2 else []) + ([2] if group >= 4 else [])
    relays = [(1, 0, 2), (2, 1, 1)] if group >= 4 else []

    def direct_copy(ph, bits, p, sending):
        return remote(own_piece(ph, p), piece(ph, t, q if sending else flip(q, bits), p),
                      ag_send.at[ph, bits, p], ag_recv.at[ph, bits, p], (z * group + flip(q, bits), t))

    def relay_copy(ph, origin, sub, to, p, sending):
        part = piece(ph, t, flip(q, origin if sending else 3), p, sub)
        return remote(part, part, ag_send.at[ph, 3 + sub, p], ag_recv.at[ph, 3 + sub, p],
                      (z * group + flip(q, to), t))

    def pair_copy(ph, bits, p, d, tt):
        qq = flip(q, bits)
        src = own_piece(ph, p) if bits == 0 else piece(ph, t, qq, p)
        return remote(src, piece(ph, tt, qq, p), pair_send.at[ph, bits, p, d],
                      pair_recv.at[ph, bits, p, d], in_pair(d))

    def pair_start(ph, bits, p):
        for d in range(1, tps):
            pair_copy(ph, bits, p, d, t).start()

    def gather_start(ph, p):
        for bits in directs:
            direct_copy(ph, bits, p, True).start()
        pair_start(ph, 0, p)

    def gather_relay(ph, p):
        for bits in directs:
            direct_copy(ph, bits, p, False).wait_recv()
            for origin, sub, to in relays:
                if origin == bits:
                    relay_copy(ph, origin, sub, to, p, True).start()
            pair_start(ph, bits, p)

    def gather_last(ph, p):
        if relays:
            for origin, sub, to in relays:
                relay_copy(ph, origin, sub, to, p, False).wait_recv()
            pair_start(ph, 3, p)

    def gather_finish(ph, p):
        gather_last(ph, p)
        gather_paired(ph, p)

    def gather_all(ph):
        each(lambda p: gather_last(ph, p))
        each(lambda p: gather_paired(ph, p))

    def gather_paired(ph, p):
        for bits in range(group):
            for d in range(1, tps):
                pair_copy(ph, bits, p, d, (t + tps - d) % tps).wait_recv()

    def gather_sent(ph, p):
        for bits in directs:
            direct_copy(ph, bits, p, True).wait_send()
        for origin, sub, to in relays:
            relay_copy(ph, origin, sub, to, p, True).wait_send()
        for bits in range(group):
            for d in range(1, tps):
                pair_copy(ph, bits, p, d, t).wait_send()

    def token_copy(p):
        return remote(own_piece(0, p), piece(2 * depth, t, q, p), tok_send.at[p], tok_recv.at[p], (partner, t))

    def gate_copy(p):
        return remote(gsend.at[pl.ds(pl.multiple_of(p * tile, tile), tile), :], piece(1, t, q, p),
                      gate_send.at[p], gate_recv.at[p], (partner, t))

    def at_tile(p):
        return pl.ds(pl.multiple_of(p * tile, tile), tile)

    def normalize(slot, l, p):
        sub = min(128, tile)

        def step(i, carry):
            at = pl.ds(pl.multiple_of(p * tile + i * sub, sub), sub)
            x = acts[slot, at, :].astype(F32)
            scale = lax.rsqrt(jnp.mean(x * x, axis=-1, keepdims=True) + 1e-06)
            normed[slot // guest, at, :] = (x * scale * gain[pl.ds(l, 1), :]).astype(BF16)
            return carry

        lax.fori_loop(0, tile // sub, step, 0)

    def project(slot, l, m, p):
        return jnp.dot(normed[slot // guest, at_tile(p), :], weights[l, m], preferred_element_type=F32).astype(BF16)

    def halo_copy(l):
        return remote(product.at[l, pl.ds(span, 8), :], product.at[l, pl.ds(0, 8), :],
                      halo_send.at[l], halo_recv.at[l], (sp + group, t))

    def do_cgate(slot, l, p):
        cgate[at_tile(p), :] = project(slot, l, 0, p)

    def do_values(slot, l, p):
        values = project(slot, l, 1, p)
        product[slot, pl.ds(pl.multiple_of(p * tile + 8, 8), tile), :] = (
            cgate[at_tile(p), :].astype(F32) * values.astype(F32))

    def do_bgate(slot, l, p):
        tap = [taps[l, pl.ds(k, 1), pl.ds(own, width)] for k in range(3)]
        bgate = project(slot, l, 2, p).astype(F32)
        near = product[slot, pl.ds(pl.multiple_of(p * tile, 8), tile + 8), :]
        mixed = tap[0] * near[6:6 + tile] + tap[1] * near[7:7 + tile] + tap[2] * near[8:8 + tile]
        return (bgate * mixed).astype(BF16)

    def no_halo(slot):
        product[slot, pl.ds(0, 8), :] = jnp.zeros((8, width), F32)

    def halo_sender(l):
        return (z >= 1) & (z < line - 2) if lend and l == 0 else z < line - 1

    def halo_taker(l):
        return (z >= 2) & (z < line - 1) if lend and l == 0 else z > 0

    def halo_start(l):
        @pl.when(halo_sender(l))
        def _():
            halo_copy(l).start()

    def halo_ready(l):
        @pl.when(halo_taker(l))
        def _():
            halo_copy(l).wait_recv()

        @pl.when(z == 0)
        def _():
            no_halo(l)

    def do_out(l, p):
        update = jnp.dot(gates[l, at_tile(p), :], weights[l, 3], preferred_element_type=F32)
        return (acts[l, at_tile(p), pl.ds(own, width)].astype(F32) + update).astype(BF16)

    per_owner = rows // tile

    def out_copy(p, sender, owner):
        return remote(result.at[at_tile(p), :],
                      landed.at[pl.ds(pl.multiple_of(p * tile % rows, tile), tile),
                                pl.ds(pl.multiple_of(sender * width, width), width)],
                      out_send.at[p], out_recv.at[sender, p], (z * group + owner, t))

    def own_gate(l, p):
        gates[l, at_tile(p), pl.ds(own, width)] = do_bgate(l, l, p)
        gather_start(2 * l + 1, p)

    guests = 2 * depth
    own_tokens = pltpu.make_async_copy(tok, acts.at[0, pl.ds(pl.multiple_of(q * rows, rows), rows), pl.ds(pl.multiple_of(t * cols, cols), cols)], loc_sem.at[last])
    own_tokens.start()

    @functools.partial(only, end)
    def _():
        each(lambda p: token_copy(p).start())

    rest = range(3, last)

    @functools.partial(only, end)
    def _():
        for i in range(last):
            plane_start(i)
        each(lambda p: gather_start(0, p))
        for i in range(last):
            line_start(i)
            if i in rest:
                raw_take(i)
        own_tokens.wait()
        each(lambda p: gather_relay(0, p))
        gather_all(0)

    @unless_end
    def _():
        for i in range(3):
            plane_start(i)

        @functools.partial(only, host)
        def _():
            for i in rest:
                for d in range(group):
                    raw_copy(i, d).start()

        line_start(0)

        @functools.partial(only, host)
        def _():
            def take(p):
                token_copy(p).wait_recv()
                gather_start(guests, p)
            each(take)

        line_start(1)
        line_start(2)

        @functools.partial(only, host)
        def _():
            gather_relay(guests, 0)
            gather_relay(guests, 1)

        inward(0)

        @functools.partial(only, host)
        def _():
            gather_relay(guests, 2)
            gather_relay(guests, 3)

        each(lambda p: gather_start(0, p))
        plane_start(3)
        inward(1)
        own_tokens.wait()

        @functools.partial(only, host)
        def _():
            gather_all(guests)
            each(lambda p: normalize(guest, 0, p))

        inward(2)
        outward(0)

        @functools.partial(only, host)
        def _():
            each(lambda p: do_cgate(guest, 0, p))

        outward(1)

        @functools.partial(only, host)
        def _():
            each(lambda p: do_values(guest, 0, p))

        each(lambda p: gather_relay(0, p))
        for i in range(4, last):
            plane_start(i)
        inward(3)
        outward(2)

        def lend_gate(p):
            gsend[at_tile(p), :] = do_bgate(guest, 0, p)
            gate_copy(p).start()

        @functools.partial(only, host)
        def _():
            lax.fori_loop(1, PIECES, lambda p, c: (lend_gate(p), c)[1], 0)

        line_start(3)

        gather_all(0)

        def take(p):
            normalize(0, 0, p)
            do_cgate(0, 0, p)
            do_values(0, 0, p)
        each(take)
        halo_start(0)

        @functools.partial(only, host)
        def _():
            @pl.when(z == 1)
            def _():
                no_halo(guest)
                product[0, pl.ds(0, 8), :] = product[guest, pl.ds(span, 8), :]

            @pl.when(z != 1)
            def _():
                product[guest, pl.ds(0, 8), :] = product[0, pl.ds(span, 8), :]

            lend_gate(0)

        inward(4)
        line_start(4)
        outward(3)
        lax.fori_loop(1, PIECES, lambda p, c: (own_gate(0, p), c)[1], 0)
        halo_ready(0)
        own_gate(0, 0)
        for i in range(5, last):
            inward(i)
            line_start(i)

    @functools.partial(only, end)
    def _():
        def take(p):
            gate_copy(p).wait_recv()
            gather_start(1, p)
        take(1)
        take(2)
        gather_relay(1, 1)
        take(3)
        gather_relay(1, 2)
        gather_relay(1, 3)
        take(0)
        outward(3)

    for l in range(depth):
        ph = 2 * l + 1
        if l + 1 < depth:
            def relay_next(k, p):
                on = k < PIECES - 1
                if l == 0 and lend:
                    on = on & (jnp.logical_not(end) | (k == PIECES - 2))

                @pl.when(on)
                def _():
                    gather_relay(ph, (p + 1) % PIECES)

            @unless_end
            def _():
                gather_relay(ph, 1)

            def forward(k):
                p = (k + 1) % PIECES
                relay_next(k, p)

                gather_finish(ph, p)
                acts[l + 1, at_tile(p), pl.ds(own, width)] = do_out(l, p)
                gather_start(ph + 1, p)

                @unless_end
                def _():
                    for n in range(2):
                        @pl.when(k == 2 * n)
                        def _():
                            outward(4 * l + 4 + n)
            each(forward)
            gather_relay(ph + 1, 1)

            def enter(k):
                p = (k + 1) % PIECES

                @pl.when(k < PIECES - 1)
                def _():
                    gather_relay(ph + 1, (p + 1) % PIECES)

                gather_finish(ph + 1, p)
                normalize(l + 1, l + 1, p)

                @unless_end
                def _():
                    @pl.when(k == 1)
                    def _():
                        outward(4 * l + 6)
            each(enter)

            @functools.partial(only, end)
            def _():
                outward(4 * l + 4)
            each(lambda p: do_cgate(l + 1, l + 1, p))

            @functools.partial(only, end)
            def _():
                outward(4 * l + 5)
            each(lambda p: do_values(l + 1, l + 1, p))
            halo_start(l + 1)

            @functools.partial(only, end)
            def _():
                outward(4 * l + 6)

            @unless_end
            def _():
                outward(4 * l + 7)
            lax.fori_loop(1, PIECES, lambda p, c: (own_gate(l + 1, p), c)[1], 0)
            halo_ready(l + 1)
            own_gate(l + 1, 0)
            gather_relay(ph + 2, 1)

            @functools.partial(only, end)
            def _():
                outward(4 * l + 7)
        else:
            def finish(k):
                p = (k + 1) % PIECES

                @pl.when(k < PIECES - 1)
                def _():
                    gather_relay(ph, (p + 1) % PIECES)

                gather_finish(ph, p)
                final = do_out(l, p)
                owner = p * tile // rows

                @pl.when(owner == q)
                def _():
                    landed[pl.ds(pl.multiple_of(p * tile % rows, tile), tile),
                           pl.ds(pl.multiple_of(q * width, width), width)] = final

                @pl.when(owner != q)
                def _():
                    result[at_tile(p), :] = final
                    out_copy(p, q, owner).start()
            each(finish)

    for d in range(1, group):
        for k in range(per_owner):
            out_copy(q * per_owner + k, (q + d) % group, q).wait_recv()
    out[...] = landed[...]

    for i in range(last):
        for d in range(1, group):
            plane_copy(i, d, q).wait_send()

        def step(zz, carry):
            for up in (True, False):
                @pl.when(goes(i, zz, up) & ((zz <= z) if up else (zz >= z)))
                def _():
                    line_copy(i, zz, up).wait_send()

            return carry

        lax.fori_loop(0, line, step, 0)
    for ph in range(2 * depth):
        each(lambda p: gather_sent(ph, p))

    @functools.partial(only, host)
    def _():
        each(lambda p: gather_sent(2 * depth, p))
        each(lambda p: gate_copy(p).wait_send())
        for i in rest:
            for d in range(group):
                raw_copy(i, d).wait_send()

    @functools.partial(only, end)
    def _():
        each(lambda p: token_copy(p).wait_send())
        for i in rest:
            for d in range(1, group):
                guest_copy(i, d, q).wait_send()

    for l in range(depth):
        @pl.when(halo_sender(l))
        def _():
            halo_copy(l).wait_send()

    def sent(p):
        owner = p * tile // rows

        @pl.when(owner != q)
        def _():
            out_copy(p, q, owner).wait_send()
    each(sent)


def shards(sp_size, tps, tokens, norm_gain, w_bgate, w_cgate, w_value, conv_taps, w_out):
    rows, cols = tokens.shape
    depth, krows, _ = w_bgate.shape
    group = 4
    while group > 1 and (sp_size % group or cols % (group * LANES)):
        group //= 2
    line = sp_size // group
    width = cols // group
    span = rows * group
    full = krows * sp_size
    n = 4 * depth
    phases = 2 * depth + 1
    dims = (depth, group, line, tps, rows, cols, width, krows)
    anywhere = pl.BlockSpec(memory_space=pl.ANY)
    vmem = pl.BlockSpec(memory_space=pltpu.VMEM)
    dma = pltpu.SemaphoreType.DMA
    return pl.pallas_call(
        functools.partial(mixer_kernel, dims),
        out_shape=jax.ShapeDtypeStruct((rows, cols), BF16),
        in_specs=[anywhere, vmem, anywhere, anywhere, anywhere, vmem, anywhere],
        out_specs=vmem,
        scratch_shapes=[
            pltpu.VMEM((depth + 1, span, full), BF16),
            pltpu.VMEM((depth, span, full), BF16),
            pltpu.VMEM((2, span, full), BF16),
            pltpu.VMEM((depth, 4, full, width), BF16),
            pltpu.VMEM((depth + 1, span + 8, width), F32),
            pltpu.VMEM((span, width), BF16),
            pltpu.VMEM((span, width), BF16),
            pltpu.VMEM((span, width), BF16),
            pltpu.VMEM((rows, cols), BF16),
            dma((n + 1,)), dma((n, group)), dma((n, group)),
            dma((2, n, line)), dma((n, line)),
            dma((phases, 5, PIECES)), dma((phases, 5, PIECES)),
            dma((phases, group, PIECES, tps)), dma((phases, group, PIECES, tps)),
            dma((depth,)), dma((depth,)), dma((PIECES,)), dma((group, PIECES)),
            dma((PIECES,)), dma((PIECES,)), dma((PIECES,)), dma((PIECES,)),
            pltpu.VMEM((n, group - 1, krows, width), BF16),
            dma((n, group)), dma((n, group)), dma((n, group)), dma((n, group)),
        ],
        compiler_params=pltpu.CompilerParams(
            collective_id=0, has_side_effects=True, vmem_limit_bytes=60 * 1024 * 1024),
    )(tokens, norm_gain, w_bgate, w_cgate, w_value, conv_taps, w_out)


def solution(mesh):
    return jax.shard_map(
        functools.partial(shards, mesh.shape["sp"], mesh.shape["tp"]),
        mesh=mesh,
        in_specs=(
            P("sp", "tp"),
            P(),
            P(None, "sp", "tp"),
            P(None, "sp", "tp"),
            P(None, "sp", "tp"),
            P(),
            P(None, "sp", "tp"),
        ),
        out_specs=P("sp", "tp"),
        check_vma=False,
    )
```

time: 187 us -> 162 us (0.87)
  Pallas kernels: 183 us -> 159 us
    pallas_call x1, Pallas kernels: 183 us -> 159 us  [shards(): pl.pallas_call(functools.partial(mixer_kernel, dims), out_shape=jax.Shape...]
where the time goes in v1:
time: 162 us
  Pallas kernels  159 us (98%)
  local copies, waits for them, and re-layouts  3.33 us (2%)
    pallas_call x1, Pallas kernels, shards(): pl.pallas_call(functools.partial(mixer_kernel, dims), out_shape=jax.Shape...  159 us
    unnamed x2, local copies, waits for them, and re-layouts  3.33 us

profile of v1, /device:TPU:0, one launch (start us, length us, event | category | flops | bytes accessed | tf_op | source)
XLA Modules:
  0.0 162.1 jit_solution(9782924134438471746)
XLA Ops:
  0.0 1.5 copy.8.taps
  1.5 158.8 %shard_map.73 = bf16[256,1024]{1,0:T(8,128)(2,1)} custom-call(bf16[256,1024]{1,0:T(8,128)(2,1)} %tok.1, f32[2,2048]{1,0:T(2,128)} %gain.1, bf16[2,128,1024]{2,1,0:T(8,128)(2,1)} %wb.1, bf16[2,128,1024]{2,1,0:T(8,128)(2,1)} %wc.1, bf16[2,128,1024]{2,1,0:T(8,128)(2,1)} %wv.1, f32[2,3,2048]{2,1,0:T(4,128)} %copy.8.taps, bf16[2,128,1024]{2,1,0:T(8,128)(2,1)} %wo.1), custom_call_target="tpu_custom_call" | custom-call | tf_op jit(solution)/shard_map/pallas_call | solution.py:675
  160.3 1.9 %copy.10 = bf16[256,1024]{1,0:T(8,128)(2,1)} copy(bf16[256,1024]{1,0:T(8,128)(2,1)} %shard_map.73) | data formatting | bytes 1048576

commit v2 on v1

--- a/solution.py
+++ b/solution.py
@@ -100,16 +100,20 @@
 
     def plane_copy(i, d, sender):
         return remote(weight_source(i, (q + d) % group), weight_rows(i, z, sender),
-                      plane_send.at[i, d], plane_recv.at[i, d], in_plane(d))
+                      plane_send, plane_recv.at[i], in_plane(d))
 
     def local_copy(i):
         return pltpu.make_async_copy(weight_source(i, q), weight_rows(i, z, q), loc_sem.at[i])
 
     low = 2 * z < line
 
+    def share(i):
+        l, m = chunks[i]
+        return l if l == 0 and m < 3 else l + 1 if l else 1
+
     def line_copy(i, zz, up):
         blk = weight_block(i, zz)
-        return remote(blk, blk, line_send.at[jnp.where(up, 0, 1), i, zz], line_recv.at[i, zz],
+        return remote(blk, blk, line_send.at[jnp.where(up, 0, 1), share(i), zz], line_recv.at[i, zz],
                       (jnp.where(up, sp + group, sp - group), t))
 
     def lent(i):
@@ -133,8 +137,9 @@
 
     def line_start(i):
         local_copy(i).wait()
-        for d in range(1, group):
-            plane_copy(i, d, (q + group - d) % group).wait_recv()
+        if group > 1:
+            ref = some_rows(i, group - 1)
+            remote(ref, ref, plane_send, plane_recv.at[i], in_plane(1)).wait_recv()
         for up in (low, jnp.logical_not(low)):
             @pl.when(goes(i, z, up))
             def _():
@@ -169,28 +174,26 @@
         if lend and not lent(i):
             @functools.partial(only, end)
             def _():
-                for d in range(1, group):
-                    guest_copy(i, d, (q + group - d) % group).wait_recv()
+                if group > 1:
+                    ref = some_rows(i, group - 1)
+                    remote(ref, ref, guest_send.at[i], guest_recv.at[i], in_plane(1)).wait_recv()
 
     def raw_copy(i, d):
         dst = weight_rows(i, z, q) if d == 0 else raw.at[i, d - 1]
-        return remote(weight_source(i, (q + d) % group), dst, raw_send.at[i, d], raw_recv.at[i, d], (partner, t))
+        return remote(weight_source(i, (q + d) % group), dst, raw_send.at[i], raw_recv.at[i], (partner, t))
 
     def host_z():
         return jnp.where(z == 0, 1, line - 2)
 
     def guest_copy(i, d, sender):
         return remote(raw.at[i, d - 1], weight_rows(i, host_z(), sender),
-                      guest_send.at[i, d], guest_recv.at[i, d], in_plane(d))
+                      guest_send.at[i], guest_recv.at[i], in_plane(d))
 
     def raw_take(i):
-        for d in range(group):
-            if d == 0:
-                remote(weight_source(i, q), weight_rows(i, host_z(), q), raw_send.at[i, 0], raw_recv.at[i, 0],
-                       (partner, t)).wait_recv()
-            else:
-                raw_copy(i, d).wait_recv()
-                guest_copy(i, d, q).start()
+        ref = some_rows(i, group)
+        remote(ref, ref, raw_send.at[i], raw_recv.at[i], (partner, t)).wait_recv()
+        for d in range(1, group):
+            guest_copy(i, d, q).start()
 
     by_rows = (0, 2 * depth)
 
@@ -223,18 +226,18 @@
 
     def direct_copy(ph, bits, p, sending):
         return remote(own_piece(ph, p), piece(ph, t, q if sending else flip(q, bits), p),
-                      ag_send.at[ph, bits, p], ag_recv.at[ph, bits, p], (z * group + flip(q, bits), t))
+                      ag_send.at[ph], ag_recv.at[ph, bits - 1, p], (z * group + flip(q, bits), t))
 
     def relay_copy(ph, origin, sub, to, p, sending):
         part = piece(ph, t, flip(q, origin if sending else 3), p, sub)
-        return remote(part, part, ag_send.at[ph, 3 + sub, p], ag_recv.at[ph, 3 + sub, p],
+        return remote(part, part, ag_send.at[ph], ag_recv.at[ph, 2, p],
                       (z * group + flip(q, to), t))
 
     def pair_copy(ph, bits, p, d, tt):
         qq = flip(q, bits)
         src = own_piece(ph, p) if bits == 0 else piece(ph, t, qq, p)
-        return remote(src, piece(ph, tt, qq, p), pair_send.at[ph, bits, p, d],
-                      pair_recv.at[ph, bits, p, d], in_pair(d))
+        return remote(src, piece(ph, tt, qq, p), pair_send.at[ph, d - 1],
+                      pair_recv.at[ph, p, d - 1], in_pair(d))
 
     def pair_start(ph, bits, p):
         for d in range(1, tps):
@@ -255,8 +258,8 @@
 
     def gather_last(ph, p):
         if relays:
-            for origin, sub, to in relays:
-                relay_copy(ph, origin, sub, to, p, False).wait_recv()
+            part = piece(ph, t, flip(q, 3), p)
+            remote(part, part, ag_send.at[ph], ag_recv.at[ph, 2, p], in_plane(1)).wait_recv()
             pair_start(ph, 3, p)
 
     def gather_finish(ph, p):
@@ -268,25 +271,73 @@
         each(lambda p: gather_paired(ph, p))
 
     def gather_paired(ph, p):
-        for bits in range(group):
-            for d in range(1, tps):
-                pair_copy(ph, bits, p, d, (t + tps - d) % tps).wait_recv()
-
-    def gather_sent(ph, p):
-        for bits in directs:
-            direct_copy(ph, bits, p, True).wait_send()
-        for origin, sub, to in relays:
-            relay_copy(ph, origin, sub, to, p, True).wait_send()
-        for bits in range(group):
-            for d in range(1, tps):
-                pair_copy(ph, bits, p, d, t).wait_send()
+        for d in range(1, tps):
+            if ph in by_rows:
+                ref = acts.at[0, pl.ds(0, span // PIECES), pl.ds(0, cols)]
+            else:
+                ref = acts.at[0, pl.ds(0, tile), pl.ds(0, cols)]
+            remote(ref, ref, pair_send.at[ph, d - 1], pair_recv.at[ph, p, d - 1], in_pair(d)).wait_recv()
+
+    def all_sent(ref, sem):
+        remote(ref, ref, sem, sem, in_pair(1)).wait_send()
+
+    def gather_sent(ph):
+        k = len(directs) + len(relays) // 2
+        if k:
+            all_sent(acts.at[0, pl.ds(0, k * rows), pl.ds(0, cols)] if ph in by_rows
+                     else acts.at[0, pl.ds(0, span), pl.ds(0, k * width)], ag_send.at[ph])
+        for d in range(1, tps):
+            all_sent(acts.at[0, pl.ds(0, span), pl.ds(0, cols)], pair_send.at[ph, d - 1])
+
+    def plane_sent():
+        if group > 1:
+            all_sent(weights.at[:, :, pl.ds(0, (group - 1) * krows), :], plane_send)
+
+    def some_rows(i, pieces):
+        l, m = chunks[i]
+        return weights.at[l, m, pl.ds(0, pieces * krows), :]
+
+    def line_sent(batch):
+        l, m = chunks[batch[0]]
+        ref = weights.at[l, pl.ds(m, len(batch)), pl.ds(0, block), :]
+
+        def step(zz, carry):
+            for up in (True, False):
+                @pl.when(goes(batch[0], zz, up) & ((zz <= z) if up else (zz >= z)))
+                def _():
+                    all_sent(ref, line_send.at[0 if up else 1, share(batch[0]), zz])
+
+            return carry
+
+        lax.fori_loop(0, line, step, 0)
+
+    def early_sent():
+        plane_sent()
+        gather_sent(0)
+        gather_sent(1)
+        line_sent(range(3))
+        line_sent(range(3, 4))
+
+        @functools.partial(only, host)
+        def _():
+            gather_sent(guests)
+            all_sent(gsend, gate_send)
+            for i in rest:
+                all_sent(some_rows(i, group), raw_send.at[i])
+
+        @functools.partial(only, end)
+        def _():
+            all_sent(acts.at[0, pl.ds(0, rows), pl.ds(0, cols)], tok_send)
+            for i in rest:
+                if group > 1:
+                    all_sent(some_rows(i, group - 1), guest_send.at[i])
 
     def token_copy(p):
-        return remote(own_piece(0, p), piece(2 * depth, t, q, p), tok_send.at[p], tok_recv.at[p], (partner, t))
+        return remote(own_piece(0, p), piece(2 * depth, t, q, p), tok_send, tok_recv.at[p], (partner, t))
 
     def gate_copy(p):
         return remote(gsend.at[pl.ds(pl.multiple_of(p * tile, tile), tile), :], piece(1, t, q, p),
-                      gate_send.at[p], gate_recv.at[p], (partner, t))
+                      gate_send, gate_recv.at[p], (partner, t))
 
     def at_tile(p):
         return pl.ds(pl.multiple_of(p * tile, tile), tile)
@@ -319,7 +370,7 @@
             cgate[at_tile(p), :].astype(F32) * values.astype(F32))
 
     def do_bgate(slot, l, p):
-        tap = [taps[l, pl.ds(k, 1), pl.ds(own, width)] for k in range(3)]
+        tap = [taps[k, pl.ds(l, 1), pl.ds(own, width)] for k in range(3)]
         bgate = project(slot, l, 2, p).astype(F32)
         near = product[slot, pl.ds(pl.multiple_of(p * tile, 8), tile + 8), :]
         mixed = tap[0] * near[6:6 + tile] + tap[1] * near[7:7 + tile] + tap[2] * near[8:8 + tile]
@@ -358,7 +409,7 @@
         return remote(result.at[at_tile(p), :],
                       landed.at[pl.ds(pl.multiple_of(p * tile % rows, tile), tile),
                                 pl.ds(pl.multiple_of(sender * width, width), width)],
-                      out_send.at[p], out_recv.at[sender, p], (z * group + owner, t))
+                      out_send, out_recv, (z * group + owner, t))
 
     def own_gate(l, p):
         gates[l, at_tile(p), pl.ds(own, width)] = do_bgate(l, l, p)
@@ -460,8 +511,13 @@
             lax.fori_loop(1, PIECES, lambda p, c: (lend_gate(p), c)[1], 0)
 
         line_start(3)
-
-        gather_all(0)
+        inward(4)
+
+        each(lambda p: gather_last(0, p))
+        outward(3)
+        line_start(4)
+        inward(5)
+        each(lambda p: gather_paired(0, p))
 
         def take(p):
             normalize(0, 0, p)
@@ -483,13 +539,11 @@
 
             lend_gate(0)
 
-        inward(4)
-        line_start(4)
-        outward(3)
+        line_start(5)
         lax.fori_loop(1, PIECES, lambda p, c: (own_gate(0, p), c)[1], 0)
         halo_ready(0)
         own_gate(0, 0)
-        for i in range(5, last):
+        for i in range(6, last):
             inward(i)
             line_start(i)
 
@@ -527,69 +581,69 @@
                 p = (k + 1) % PIECES
                 relay_next(k, p)
 
+                @unless_end
+                def _():
+                    for n in range(2):
+                        @pl.when(k == (0, PIECES - 1)[n])
+                        def _():
+                            outward(4 * l + 4 + n)
+
                 gather_finish(ph, p)
                 acts[l + 1, at_tile(p), pl.ds(own, width)] = do_out(l, p)
                 gather_start(ph + 1, p)
-
-                @unless_end
-                def _():
-                    for n in range(2):
-                        @pl.when(k == 2 * n)
-                        def _():
-                            outward(4 * l + 4 + n)
             each(forward)
-            gather_relay(ph + 1, 1)
-
-            def enter(k):
-                p = (k + 1) % PIECES
-
-                @pl.when(k < PIECES - 1)
-                def _():
-                    gather_relay(ph + 1, (p + 1) % PIECES)
-
-                gather_finish(ph + 1, p)
+            @unless_end
+            def _():
+                outward(4 * l + 6)
+            each(lambda k: gather_relay(ph + 1, (k + 1) % PIECES))
+
+            @functools.partial(only, end)
+            def _():
+                outward(4 * l + 4)
+                outward(4 * l + 5)
+
+            early_sent()
+
+            def enter(p):
+                gather_paired(ph + 1, p)
                 normalize(l + 1, l + 1, p)
-
-                @unless_end
-                def _():
-                    @pl.when(k == 1)
-                    def _():
-                        outward(4 * l + 6)
-            each(enter)
+                do_cgate(l + 1, l + 1, p)
+                do_values(l + 1, l + 1, p)
+
+            gather_last(ph + 1, 1)
+            gather_last(ph + 1, 2)
+            enter(1)
+            gather_last(ph + 1, 3)
+            enter(2)
 
             @functools.partial(only, end)
             def _():
-                outward(4 * l + 4)
-            each(lambda p: do_cgate(l + 1, l + 1, p))
-
-            @functools.partial(only, end)
-            def _():
-                outward(4 * l + 5)
-            each(lambda p: do_values(l + 1, l + 1, p))
+                outward(4 * l + 6)
+            own_gate(l + 1, 2)
+            gather_last(ph + 1, 0)
+            enter(3)
             halo_start(l + 1)
-
-            @functools.partial(only, end)
-            def _():
-                outward(4 * l + 6)
+            own_gate(l + 1, 3)
 
             @unless_end
             def _():
                 outward(4 * l + 7)
-            lax.fori_loop(1, PIECES, lambda p, c: (own_gate(l + 1, p), c)[1], 0)
+            enter(0)
+            own_gate(l + 1, 1)
             halo_ready(l + 1)
             own_gate(l + 1, 0)
-            gather_relay(ph + 2, 1)
+            gather_relay(ph + 2, 2)
 
             @functools.partial(only, end)
             def _():
                 outward(4 * l + 7)
         else:
             def finish(k):
-                p = (k + 1) % PIECES
+                p = jnp.where(k < 2, k + 2, 3 - k)
 
                 @pl.when(k < PIECES - 1)
                 def _():
-                    gather_relay(ph, (p + 1) % PIECES)
+                    gather_relay(ph, jnp.where(k < 1, 3, 2 - k))
 
                 gather_finish(ph, p)
                 final = do_out(l, p)
@@ -606,54 +660,23 @@
                     out_copy(p, q, owner).start()
             each(finish)
 
-    for d in range(1, group):
-        for k in range(per_owner):
-            out_copy(q * per_owner + k, (q + d) % group, q).wait_recv()
+    if group > 1:
+        ref = landed.at[:, pl.ds(0, (group - 1) * width)]
+        remote(ref, ref, out_send, out_recv, in_plane(1)).wait_recv()
     out[...] = landed[...]
 
-    for i in range(last):
-        for d in range(1, group):
-            plane_copy(i, d, q).wait_send()
-
-        def step(zz, carry):
-            for up in (True, False):
-                @pl.when(goes(i, zz, up) & ((zz <= z) if up else (zz >= z)))
-                def _():
-                    line_copy(i, zz, up).wait_send()
-
-            return carry
-
-        lax.fori_loop(0, line, step, 0)
-    for ph in range(2 * depth):
-        each(lambda p: gather_sent(ph, p))
-
-    @functools.partial(only, host)
-    def _():
-        each(lambda p: gather_sent(2 * depth, p))
-        each(lambda p: gate_copy(p).wait_send())
-        for i in rest:
-            for d in range(group):
-                raw_copy(i, d).wait_send()
-
-    @functools.partial(only, end)
-    def _():
-        each(lambda p: token_copy(p).wait_send())
-        for i in rest:
-            for d in range(1, group):
-                guest_copy(i, d, q).wait_send()
+    for l in range(1, depth):
+        line_sent(range(4 * l, 4 * l + 4))
+    for ph in range(2, 2 * depth):
+        gather_sent(ph)
 
     for l in range(depth):
         @pl.when(halo_sender(l))
         def _():
             halo_copy(l).wait_send()
 
-    def sent(p):
-        owner = p * tile // rows
-
-        @pl.when(owner != q)
-        def _():
-            out_copy(p, q, owner).wait_send()
-    each(sent)
+    if group > 1:
+        all_sent(result.at[pl.ds(0, (PIECES - per_owner) * tile), :], out_send)
 
 
 def shards(sp_size, tps, tokens, norm_gain, w_bgate, w_cgate, w_value, conv_taps, w_out):
@@ -668,6 +691,7 @@
     full = krows * sp_size
     n = 4 * depth
     phases = 2 * depth + 1
+    others = max(1, tps - 1)
     dims = (depth, group, line, tps, rows, cols, width, krows)
     anywhere = pl.BlockSpec(memory_space=pl.ANY)
     vmem = pl.BlockSpec(memory_space=pltpu.VMEM)
@@ -687,18 +711,18 @@
             pltpu.VMEM((span, width), BF16),
             pltpu.VMEM((span, width), BF16),
             pltpu.VMEM((rows, cols), BF16),
-            dma((n + 1,)), dma((n, group)), dma((n, group)),
-            dma((2, n, line)), dma((n, line)),
-            dma((phases, 5, PIECES)), dma((phases, 5, PIECES)),
-            dma((phases, group, PIECES, tps)), dma((phases, group, PIECES, tps)),
-            dma((depth,)), dma((depth,)), dma((PIECES,)), dma((group, PIECES)),
-            dma((PIECES,)), dma((PIECES,)), dma((PIECES,)), dma((PIECES,)),
-            pltpu.VMEM((n, group - 1, krows, width), BF16),
-            dma((n, group)), dma((n, group)), dma((n, group)), dma((n, group)),
+            dma((n + 1,)), dma(()), dma((n,)),
+            dma((2, depth + 1, line)), dma((n, line)),
+            dma((phases,)), dma((phases, 3, PIECES)),
+            dma((phases, others)), dma((phases, PIECES, others)),
+            dma((depth,)), dma((depth,)), dma(()), dma(()),
+            dma(()), dma((PIECES,)), dma(()), dma((PIECES,)),
+            pltpu.VMEM((n, max(1, group - 1), krows, width), BF16),
+            dma((n,)), dma((n,)), dma((n,)), dma((n,)),
         ],
         compiler_params=pltpu.CompilerParams(
             collective_id=0, has_side_effects=True, vmem_limit_bytes=60 * 1024 * 1024),
-    )(tokens, norm_gain, w_bgate, w_cgate, w_value, conv_taps, w_out)
+    )(tokens, norm_gain, w_bgate, w_cgate, w_value, conv_taps.transpose(1, 0, 2), w_out)
 
 
 def solution(mesh):

time: 162 us -> 154 us (0.951)
  Pallas kernels: 159 us -> 151 us
    pallas_call x1, Pallas kernels: 159 us -> 151 us  [shards(): pl.pallas_call(functools.partial(mixer_kernel, dims), out_shape=jax.Shape...]
    unnamed x2 -> x1, local copies, waits for them, and re-layouts: 3.33 us -> 1.87 us
where the time goes in v2:
time: 154 us; the launch traced here: 153 us
  Pallas kernels  151 us (98%)
  local copies, waits for them, and re-layouts  1.87 us (1%)
    pallas_call x1, Pallas kernels, shards(): pl.pallas_call(functools.partial(mixer_kernel, dims), out_shape=jax.Shape...  151 us

profile of v2, /device:TPU:0, one launch (start us, length us, event | category | flops | bytes accessed | tf_op | source)
XLA Modules:
  0.0 153.0 jit_solution(15402982303701801516)
XLA Ops:
  0.0 151.2 %shard_map.73 = bf16[256,1024]{1,0:T(8,128)(2,1)} custom-call(bf16[256,1024]{1,0:T(8,128)(2,1)} %tok.1, f32[2,2048]{1,0:T(2,128)} %gain.1, bf16[2,128,1024]{2,1,0:T(8,128)(2,1)} %wb.1, bf16[2,128,1024]{2,1,0:T(8,128)(2,1)} %wc.1, bf16[2,128,1024]{2,1,0:T(8,128)(2,1)} %wv.1, f32[3,2,2048]{2,1,0:T(2,128)} %bitcast.1, bf16[2,128,1024]{2,1,0:T(8,128)(2,1)} %wo.1), custom_call_target="tpu_custom_call" | custom-call | tf_op jit(solution)/shard_map/pallas_call | solution.py:699
  151.2 1.9 %copy.9 = bf16[256,1024]{1,0:T(8,128)(2,1)} copy(bf16[256,1024]{1,0:T(8,128)(2,1)} %shard_map.73) | data formatting | bytes 1048576

commit v3 on v2

--- a/solution.py
+++ b/solution.py
@@ -26,6 +26,7 @@
     span = rows * group
     block = krows * group
     tile = span // PIECES
+    part = rows // PIECES
     lend = line >= 4
     guest = depth
     chunks = [(l, m) for l in range(depth) for m in range(4)]
@@ -199,18 +200,18 @@
 
     def piece(ph, tt, qq, p, sub=None):
         if ph in by_rows:
-            part, slot = rows // PIECES, 0 if ph == 0 else guest
-            first, col, wide, buf = qq * rows, tt * cols, cols, acts
+            size, slot, at = part, 0 if ph == 0 else guest, p * tile + qq * part
+            col, wide, buf = tt * cols, cols, acts
         else:
-            part, slot = tile, ph // 2
-            first, col, wide, buf = 0, tt * cols + qq * width, width, acts if ph % 2 == 0 else gates
-        size = part if sub is None else part // 2
-        at = first + p * part + (0 if sub is None else sub * size)
+            size, slot, at = tile, ph // 2, p * tile
+            col, wide, buf = tt * cols + qq * width, width, acts if ph % 2 == 0 else gates
+        if sub is not None:
+            size = size // 2
+            at = at + sub * size
         return buf.at[slot, pl.ds(pl.multiple_of(at, size), size), pl.ds(pl.multiple_of(col, wide), wide)]
 
     def own_piece(ph, p):
         if ph == 0:
-            part = rows // PIECES
             return tok.at[pl.ds(pl.multiple_of(p * part, part), part), :]
         return piece(ph, t, q, p)
 
@@ -229,8 +230,8 @@
                       ag_send.at[ph], ag_recv.at[ph, bits - 1, p], (z * group + flip(q, bits), t))
 
     def relay_copy(ph, origin, sub, to, p, sending):
-        part = piece(ph, t, flip(q, origin if sending else 3), p, sub)
-        return remote(part, part, ag_send.at[ph], ag_recv.at[ph, 2, p],
+        ref = piece(ph, t, flip(q, origin if sending else 3), p, sub)
+        return remote(ref, ref, ag_send.at[ph], ag_recv.at[ph, 2, p],
                       (z * group + flip(q, to), t))
 
     def pair_copy(ph, bits, p, d, tt):
@@ -258,8 +259,8 @@
 
     def gather_last(ph, p):
         if relays:
-            part = piece(ph, t, flip(q, 3), p)
-            remote(part, part, ag_send.at[ph], ag_recv.at[ph, 2, p], in_plane(1)).wait_recv()
+            ref = piece(ph, t, flip(q, 3), p)
+            remote(ref, ref, ag_send.at[ph], ag_recv.at[ph, 2, p], in_plane(1)).wait_recv()
             pair_start(ph, 3, p)
 
     def gather_finish(ph, p):
@@ -358,7 +359,7 @@
         return jnp.dot(normed[slot // guest, at_tile(p), :], weights[l, m], preferred_element_type=F32).astype(BF16)
 
     def halo_copy(l):
-        return remote(product.at[l, pl.ds(span, 8), :], product.at[l, pl.ds(0, 8), :],
+        return remote(product.at[l, PIECES - 1, group - 1, pl.ds(part, 8), :], product.at[l, 0, 0, pl.ds(0, 8), :],
                       halo_send.at[l], halo_recv.at[l], (sp + group, t))
 
     def do_cgate(slot, l, p):
@@ -366,18 +367,32 @@
 
     def do_values(slot, l, p):
         values = project(slot, l, 1, p)
-        product[slot, pl.ds(pl.multiple_of(p * tile + 8, 8), tile), :] = (
-            cgate[at_tile(p), :].astype(F32) * values.astype(F32))
+        made = cgate[at_tile(p), :].astype(F32) * values.astype(F32)
+        for qq in range(group):
+            rows_of = made[qq * part:(qq + 1) * part]
+            product[slot, p, qq, pl.ds(8, part), :] = rows_of
+
+            @pl.when(p < PIECES - 1)
+            def _():
+                product[slot, (p + 1) % PIECES, qq, pl.ds(0, 8), :] = rows_of[part - 8:]
+
+            if qq + 1 < group:
+                @pl.when(p == PIECES - 1)
+                def _():
+                    product[slot, 0, qq + 1, pl.ds(0, 8), :] = rows_of[part - 8:]
 
     def do_bgate(slot, l, p):
         tap = [taps[k, pl.ds(l, 1), pl.ds(own, width)] for k in range(3)]
         bgate = project(slot, l, 2, p).astype(F32)
-        near = product[slot, pl.ds(pl.multiple_of(p * tile, 8), tile + 8), :]
-        mixed = tap[0] * near[6:6 + tile] + tap[1] * near[7:7 + tile] + tap[2] * near[8:8 + tile]
-        return (bgate * mixed).astype(BF16)
+        gated = []
+        for qq in range(group):
+            near = product[slot, p, qq]
+            mixed = tap[0] * near[6:6 + part] + tap[1] * near[7:7 + part] + tap[2] * near[8:8 + part]
+            gated.append((bgate[qq * part:(qq + 1) * part] * mixed).astype(BF16))
+        return jnp.concatenate(gated, axis=0)
 
     def no_halo(slot):
-        product[slot, pl.ds(0, 8), :] = jnp.zeros((8, width), F32)
+        product[slot, 0, 0, pl.ds(0, 8), :] = jnp.zeros((8, width), F32)
 
     def halo_sender(l):
         return (z >= 1) & (z < line - 2) if lend and l == 0 else z < line - 1
@@ -403,21 +418,20 @@
         update = jnp.dot(gates[l, at_tile(p), :], weights[l, 3], preferred_element_type=F32)
         return (acts[l, at_tile(p), pl.ds(own, width)].astype(F32) + update).astype(BF16)
 
-    per_owner = rows // tile
-
-    def out_copy(p, sender, owner):
-        return remote(result.at[at_tile(p), :],
-                      landed.at[pl.ds(pl.multiple_of(p * tile % rows, tile), tile),
-                                pl.ds(pl.multiple_of(sender * width, width), width)],
-                      out_send, out_recv, (z * group + owner, t))
+    def out_copy(p, d):
+        owner = (q + d) % group
+        return remote(result.at[pl.ds(pl.multiple_of(p * tile + owner * part, part), part), :],
+                      landed.at[pl.ds(pl.multiple_of(p * part, part), part),
+                                pl.ds(pl.multiple_of(q * width, width), width)],
+                      out_send, out_recv, in_plane(d))
 
     def own_gate(l, p):
         gates[l, at_tile(p), pl.ds(own, width)] = do_bgate(l, l, p)
         gather_start(2 * l + 1, p)
 
     guests = 2 * depth
-    own_tokens = pltpu.make_async_copy(tok, acts.at[0, pl.ds(pl.multiple_of(q * rows, rows), rows), pl.ds(pl.multiple_of(t * cols, cols), cols)], loc_sem.at[last])
-    own_tokens.start()
+    own_tokens = pltpu.make_async_copy(tok, acts.at[0, pl.ds(0, rows), pl.ds(0, cols)], loc_sem.at[last])
+    each(lambda p: pltpu.make_async_copy(own_piece(0, p), piece(0, t, q, p), loc_sem.at[last]).start())
 
     @functools.partial(only, end)
     def _():
@@ -480,8 +494,12 @@
 
         @functools.partial(only, host)
         def _():
-            gather_all(guests)
-            each(lambda p: normalize(guest, 0, p))
+            each(lambda p: gather_last(guests, p))
+
+            def warm(p):
+                gather_paired(guests, p)
+                normalize(guest, 0, p)
+            each(warm)
 
         inward(2)
         outward(0)
@@ -497,8 +515,8 @@
             each(lambda p: do_values(guest, 0, p))
 
         each(lambda p: gather_relay(0, p))
-        for i in range(4, last):
-            plane_start(i)
+        plane_start(4)
+        plane_start(5)
         inward(3)
         outward(2)
 
@@ -512,17 +530,21 @@
 
         line_start(3)
         inward(4)
-
-        each(lambda p: gather_last(0, p))
-        outward(3)
-        line_start(4)
-        inward(5)
-        each(lambda p: gather_paired(0, p))
+        gather_last(0, 0)
 
         def take(p):
+            @pl.when(p < PIECES - 1)
+            def _():
+                gather_last(0, p + 1)
+
+            gather_paired(0, p)
             normalize(0, 0, p)
             do_cgate(0, 0, p)
             do_values(0, 0, p)
+
+            @pl.when(p > 0)
+            def _():
+                own_gate(0, p)
         each(take)
         halo_start(0)
 
@@ -531,18 +553,23 @@
             @pl.when(z == 1)
             def _():
                 no_halo(guest)
-                product[0, pl.ds(0, 8), :] = product[guest, pl.ds(span, 8), :]
+                product[0, 0, 0, pl.ds(0, 8), :] = product[guest, PIECES - 1, group - 1, pl.ds(part, 8), :]
 
             @pl.when(z != 1)
             def _():
-                product[guest, pl.ds(0, 8), :] = product[0, pl.ds(span, 8), :]
+                product[guest, 0, 0, pl.ds(0, 8), :] = product[0, PIECES - 1, group - 1, pl.ds(part, 8), :]
 
             lend_gate(0)
 
-        line_start(5)
-        lax.fori_loop(1, PIECES, lambda p, c: (own_gate(0, p), c)[1], 0)
         halo_ready(0)
         own_gate(0, 0)
+        line_start(4)
+        inward(5)
+        for i in range(6, last):
+            plane_start(i)
+        outward(3)
+        line_start(5)
+        gather_relay(1, 1)
         for i in range(6, last):
             inward(i)
             line_start(i)
@@ -573,20 +600,19 @@
                 def _():
                     gather_relay(ph, (p + 1) % PIECES)
 
-            @unless_end
-            def _():
+            if l > 0:
                 gather_relay(ph, 1)
 
             def forward(k):
                 p = (k + 1) % PIECES
-                relay_next(k, p)
 
                 @unless_end
                 def _():
                     for n in range(2):
-                        @pl.when(k == (0, PIECES - 1)[n])
+                        @pl.when(k == 2 * n)
                         def _():
                             outward(4 * l + 4 + n)
+                relay_next(k, p)
 
                 gather_finish(ph, p)
                 acts[l + 1, at_tile(p), pl.ds(own, width)] = do_out(l, p)
@@ -616,13 +642,15 @@
             gather_last(ph + 1, 3)
             enter(2)
 
-            @functools.partial(only, end)
-            def _():
-                outward(4 * l + 6)
-            own_gate(l + 1, 2)
+            unless_end(lambda: own_gate(l + 1, 2))
             gather_last(ph + 1, 0)
             enter(3)
             halo_start(l + 1)
+
+            @functools.partial(only, end)
+            def _():
+                outward(4 * l + 6)
+                own_gate(l + 1, 2)
             own_gate(l + 1, 3)
 
             @unless_end
@@ -646,18 +674,11 @@
                     gather_relay(ph, jnp.where(k < 1, 3, 2 - k))
 
                 gather_finish(ph, p)
-                final = do_out(l, p)
-                owner = p * tile // rows
-
-                @pl.when(owner == q)
-                def _():
-                    landed[pl.ds(pl.multiple_of(p * tile % rows, tile), tile),
-                           pl.ds(pl.multiple_of(q * width, width), width)] = final
-
-                @pl.when(owner != q)
-                def _():
-                    result[at_tile(p), :] = final
-                    out_copy(p, q, owner).start()
+                result[at_tile(p), :] = do_out(l, p)
+                for d in range(1, group):
+                    out_copy(p, d).start()
+                landed[pl.ds(pl.multiple_of(p * part, part), part), pl.ds(pl.multiple_of(q * width, width), width)] = result[
+                    pl.ds(pl.multiple_of(p * tile + q * part, part), part), :]
             each(finish)
 
     if group > 1:
@@ -676,7 +697,7 @@
             halo_copy(l).wait_send()
 
     if group > 1:
-        all_sent(result.at[pl.ds(0, (PIECES - per_owner) * tile), :], out_send)
+        all_sent(result.at[pl.ds(0, (group - 1) * rows), :], out_send)
 
 
 def shards(sp_size, tps, tokens, norm_gain, w_bgate, w_cgate, w_value, conv_taps, w_out):
@@ -706,7 +727,7 @@
             pltpu.VMEM((depth, span, full), BF16),
             pltpu.VMEM((2, span, full), BF16),
             pltpu.VMEM((depth, 4, full, width), BF16),
-            pltpu.VMEM((depth + 1, span + 8, width), F32),
+            pltpu.VMEM((depth + 1, PIECES, group, rows // PIECES + 8, width), F32),
             pltpu.VMEM((span, width), BF16),
             pltpu.VMEM((span, width), BF16),
             pltpu.VMEM((span, width), BF16),

time: 154 us -> 145 us (0.942)
  Pallas kernels: 151 us -> 143 us
    pallas_call x1, Pallas kernels: 151 us -> 143 us  [shards(): pl.pallas_call(functools.partial(mixer_kernel, dims), out_shape=jax.Shape...]
where the time goes in v3:
time: 145 us
  Pallas kernels  143 us (99%)
  local copies, waits for them, and re-layouts  1.87 us (1%)
    pallas_call x1, Pallas kernels, shards(): pl.pallas_call(functools.partial(mixer_kernel, dims), out_shape=jax.Shape...  143 us

profile of v3, /device:TPU:0, one launch (start us, length us, event | category | flops | bytes accessed | tf_op | source)
XLA Modules:
  0.0 145.0 jit_solution(7823738106907674679)
XLA Ops:
  0.0 143.2 %shard_map.73 = bf16[256,1024]{1,0:T(8,128)(2,1)} custom-call(bf16[256,1024]{1,0:T(8,128)(2,1)} %tok.1, f32[2,2048]{1,0:T(2,128)} %gain.1, bf16[2,128,1024]{2,1,0:T(8,128)(2,1)} %wb.1, bf16[2,128,1024]{2,1,0:T(8,128)(2,1)} %wc.1, bf16[2,128,1024]{2,1,0:T(8,128)(2,1)} %wv.1, f32[3,2,2048]{2,1,0:T(2,128)} %bitcast.1, bf16[2,128,1024]{2,1,0:T(8,128)(2,1)} %wo.1), custom_call_target="tpu_custom_call" | custom-call | tf_op jit(solution)/shard_map/pallas_call | solution.py:720
  143.2 1.9 %copy.9 = bf16[256,1024]{1,0:T(8,128)(2,1)} copy(bf16[256,1024]{1,0:T(8,128)(2,1)} %shard_map.73) | data formatting | bytes 1048576

commit v4 on v3

--- a/solution.py
+++ b/solution.py
@@ -9,7 +9,6 @@
 
 MESH = pl.DeviceIdType.MESH
 LANES = 128
-AHEAD = 2
 PIECES = 4
 F32 = jnp.float32
 BF16 = jnp.bfloat16
@@ -146,8 +145,9 @@
             def _():
                 line_copy(i, z, up).start()
 
-    def line_pass(i, up):
+    def line_pass(i, up, js=None):
         lo, hi = reach(i)
+        j0, j1 = js or (0, line - 1)
 
         def step(j, carry):
             zz = jnp.where(up, z - 1 - j, z + 1 + j)
@@ -165,14 +165,14 @@
 
             return carry
 
-        lax.fori_loop(0, line - 1, step, 0)
+        lax.fori_loop(j0, j1, step, 0)
 
     def inward(i):
         line_pass(i, low)
 
-    def outward(i):
-        line_pass(i, jnp.logical_not(low))
-        if lend and not lent(i):
+    def outward(i, js=None):
+        line_pass(i, jnp.logical_not(low), js)
+        if js is None and lend and not lent(i):
             @functools.partial(only, end)
             def _():
                 if group > 1:
@@ -570,6 +570,7 @@
         outward(3)
         line_start(5)
         gather_relay(1, 1)
+        outward(4, (0, 1))
         for i in range(6, last):
             inward(i)
             line_start(i)
@@ -611,7 +612,7 @@
                     for n in range(2):
                         @pl.when(k == 2 * n)
                         def _():
-                            outward(4 * l + 4 + n)
+                            outward(4 * l + 4 + n, (1, line - 1) if l + n == 0 else None)
                 relay_next(k, p)
 
                 gather_finish(ph, p)
@@ -647,20 +648,22 @@
             enter(3)
             halo_start(l + 1)
 
+            @unless_end
+            def _():
+                own_gate(l + 1, 3)
+                outward(4 * l + 7)
+            enter(0)
+
             @functools.partial(only, end)
             def _():
                 outward(4 * l + 6)
                 own_gate(l + 1, 2)
-            own_gate(l + 1, 3)
-
-            @unless_end
-            def _():
-                outward(4 * l + 7)
-            enter(0)
+                own_gate(l + 1, 3)
             own_gate(l + 1, 1)
             halo_ready(l + 1)
             own_gate(l + 1, 0)
             gather_relay(ph + 2, 2)
+            gather_relay(ph + 2, 3)
 
             @functools.partial(only, end)
             def _():
@@ -669,9 +672,9 @@
             def finish(k):
                 p = jnp.where(k < 2, k + 2, 3 - k)
 
-                @pl.when(k < PIECES - 1)
+                @pl.when(k < PIECES - 2)
                 def _():
-                    gather_relay(ph, jnp.where(k < 1, 3, 2 - k))
+                    gather_relay(ph, 1 - k)
 
                 gather_finish(ph, p)
                 result[at_tile(p), :] = do_out(l, p)

time: 145 us -> 141 us (0.972)
  Pallas kernels: 143 us -> 139 us
    pallas_call x1, Pallas kernels: 143 us -> 139 us  [shards(): pl.pallas_call(functools.partial(mixer_kernel, dims), out_shape=jax.Shape...]
where the time goes in v4:
time: 141 us
  Pallas kernels  139 us (99%)
  local copies, waits for them, and re-layouts  1.87 us (1%)
    pallas_call x1, Pallas kernels, shards(): pl.pallas_call(functools.partial(mixer_kernel, dims), out_shape=jax.Shape...  139 us

profile of v4, /device:TPU:0, one launch (start us, length us, event | category | flops | bytes accessed | tf_op | source)
XLA Modules:
  0.0 141.0 jit_solution(9668218419716827980)
XLA Ops:
  0.0 139.1 %shard_map.73 = bf16[256,1024]{1,0:T(8,128)(2,1)} custom-call(bf16[256,1024]{1,0:T(8,128)(2,1)} %tok.1, f32[2,2048]{1,0:T(2,128)} %gain.1, bf16[2,128,1024]{2,1,0:T(8,128)(2,1)} %wb.1, bf16[2,128,1024]{2,1,0:T(8,128)(2,1)} %wc.1, bf16[2,128,1024]{2,1,0:T(8,128)(2,1)} %wv.1, f32[3,2,2048]{2,1,0:T(2,128)} %bitcast.1, bf16[2,128,1024]{2,1,0:T(8,128)(2,1)} %wo.1), custom_call_target="tpu_custom_call" | custom-call | tf_op jit(solution)/shard_map/pallas_call | solution.py:723
  139.1 1.9 %copy.9 = bf16[256,1024]{1,0:T(8,128)(2,1)} copy(bf16[256,1024]{1,0:T(8,128)(2,1)} %shard_map.73) | data formatting | bytes 1048576
